TPU v7x, 32 devices: a whole 2x2x4 slice. The times are simulated.
32 devices in a mesh: kv: 8 (over z, y), tp: 4 (over x, core).
Axes of the slice: x: 2, y: 2, z: 4, core: 2. Of those that a mesh axis runs over, the one named last changes fastest.
Arguments:
- tokens: bfloat16 [32, 4096], P(None, ('kv', 'tp')), may hold values from -36 to 36
- first_gain: float32 [4096], P('kv'), may hold values from 0.1 to 1.9
- first_gate: bfloat16 [4096, 11264], P('kv', 'tp'), may hold values from -0.09375 to 0.09375
- first_up: bfloat16 [4096, 11264], P('kv', 'tp'), may hold values from -0.09375 to 0.09375
- first_down: bfloat16 [11264, 4096], P('tp', 'kv'), may hold values from -0.0546875 to 0.0546875
- mix_gain: float32 [4096], P('kv'), may hold values from 0.1 to 1.9
- w_query: bfloat16 [4096, 2048], P('kv', 'tp'), may hold values from -0.09375 to 0.09375
- key_cache: bfloat16 [32, 8192, 1024], P(None, 'kv', 'tp'), may hold values from -100 to 100
- value_cache: bfloat16 [32, 8192, 1024], P(None, 'kv', 'tp'), may hold values from -6 to 6
- map_weight: float32 [32], P('tp'), may hold values from 0.3 to 0.8
- head_gain: float32 [64], replicated, may hold values from 0.1 to 1.9
- w_out: bfloat16 [2048, 4096], P('tp', 'kv'), may hold values from -0.125 to 0.125
- second_gain: float32 [4096], P('kv'), may hold values from 0.1 to 1.9
- second_gate: bfloat16 [4096, 11264], P('kv', 'tp'), may hold values from -0.09375 to 0.09375
- second_up: bfloat16 [4096, 11264], P('kv', 'tp'), may hold values from -0.09375 to 0.09375
- second_down: bfloat16 [11264, 4096], P('tp', 'kv'), may hold values from -0.0546875 to 0.0546875
Outputs:
- mixed: bfloat16 [32, 4096], P(None, ('kv', 'tp'))
All inputs are finite; a program needn't handle non-finite values.
Results may differ from a plain program's by a relative error of at most 0.0158.
Values may be sent and summed in bfloat16 or wider, within the bound.
A program may use at most 128 MiB of HBM per device.

v0:
```python
import math
import jax
import jax.numpy as jnp
from jax import lax
from jax.sharding import PartitionSpec as P

D = 4096
HEAD = 64
EPS = 1e-06
HEAD_SCALE = 0.8


def merged(value, axis, join):
    pieces = jax.tree.map(lambda part: lax.all_gather(part, axis), value)
    head = jax.tree.map(lambda part: part[0], pieces)
    tail = jax.tree.map(lambda part: part[1:], pieces)
    subtotal, _ = lax.scan(lambda subtotal, piece: (join(subtotal, piece), None), head, tail)
    return subtotal


def norm_total(squares):
    return lax.psum(squares, "kv")


def channel_mixer(residual, gain, w_gate, w_up, w_down):
    squares = jnp.sum(residual * residual, axis=1, keepdims=True)
    scaled = (residual * gain).astype(jnp.bfloat16)
    part_gate = jnp.dot(scaled, w_gate, preferred_element_type=jnp.float32)
    part_up = jnp.dot(scaled, w_up, preferred_element_type=jnp.float32)
    row_total = norm_total(squares)
    gate_sum, up_sum = lax.psum((part_gate, part_up), "kv")
    factor = lax.rsqrt(row_total / D + EPS)
    active = (jax.nn.silu(gate_sum * factor) * (up_sum * factor)).astype(jnp.bfloat16)
    partial_value = jnp.dot(active, w_down, preferred_element_type=jnp.float32)
    return lax.psum(partial_value, "tp")


def merge_pair(first, second):
    row_peak = jnp.maximum(first[0], second[0])
    scale_first = jnp.exp(first[0] - row_peak)
    scale_second = jnp.exp(second[0] - row_peak)
    return (
        row_peak,
        first[1] * scale_first + second[1] * scale_second,
        first[2] * scale_first[..., None] + second[2] * scale_second[..., None],
    )


def combine_maps(earlier, later):
    return merge_pair(earlier[:3], later[:3]) + merge_pair(earlier[3:], later[3:])


def attention_mix(
    residual, mix_gain, w_query, key_cache, value_cache, map_weight, head_gain, w_out
):
    squares = jnp.sum(residual * residual, axis=1, keepdims=True)
    scaled = (residual * mix_gain).astype(jnp.bfloat16)
    part_query = jnp.dot(scaled, w_query, preferred_element_type=jnp.float32)
    row_total = norm_total(squares)
    queries = lax.psum(part_query, "kv")
    queries = (queries * lax.rsqrt(row_total / D + EPS)).astype(jnp.bfloat16)
    batch_rows = queries.shape[0]
    kv_local = key_cache.shape[2] // HEAD
    group = queries.shape[1] // (kv_local * HEAD)
    queries = queries.reshape(batch_rows, kv_local, group, HEAD)
    cached = key_cache.reshape(batch_rows, -1, kv_local, HEAD)
    stored = value_cache.reshape(batch_rows, -1, kv_local, HEAD)

    def partial_map(first_col, last_col):
        scores = jnp.einsum(
            "bkgd,bpkd->bkgp",
            queries[..., first_col:last_col],
            cached[..., first_col:last_col],
            preferred_element_type=jnp.float32,
        ) / math.sqrt(last_col - first_col)
        row_peak = jnp.max(scores, axis=3)
        exp_terms = jnp.exp(scores - row_peak[..., None])
        weights_sum = jnp.sum(exp_terms, axis=3)
        summed = jnp.einsum(
            "bkgp,bpkd->bkgd",
            exp_terms.astype(jnp.bfloat16),
            stored,
            preferred_element_type=jnp.float32,
        )
        return (row_peak, weights_sum, summed)

    half_dim = HEAD // 2
    peak_one, sum_one, out_one = partial_map(0, half_dim)
    peak_two, sum_two, out_two = partial_map(half_dim, HEAD)
    peak_one, sum_one, out_one, peak_two, sum_two, out_two = merged(
        (peak_one, sum_one, out_one, peak_two, sum_two, out_two), "kv", combine_maps
    )
    weight = map_weight.reshape(kv_local, group)
    combined = out_one / sum_one[..., None] - weight[..., None] * out_two / sum_two[..., None]
    normed = (
        combined
        * lax.rsqrt(jnp.mean(combined * combined, axis=3, keepdims=True) + EPS)
        * head_gain
        * HEAD_SCALE
    )
    normed = normed.astype(jnp.bfloat16).reshape(batch_rows, kv_local * group * HEAD)
    partial_value = jnp.dot(normed, w_out, preferred_element_type=jnp.float32)
    return lax.psum(partial_value, "tp")


def on_device(
    tokens,
    first_gain,
    first_gate,
    first_up,
    first_down,
    mix_gain,
    w_query,
    key_cache,
    value_cache,
    map_weight,
    head_gain,
    w_out,
    second_gain,
    second_gate,
    second_up,
    second_down,
):
    residual = lax.all_gather(tokens, "tp", axis=1, tiled=True).astype(jnp.float32)
    residual = residual + 0.5 * channel_mixer(
        residual, first_gain, first_gate, first_up, first_down
    )
    residual = residual + attention_mix(
        residual, mix_gain, w_query, key_cache, value_cache, map_weight, head_gain, w_out
    )
    residual = residual + 0.5 * channel_mixer(
        residual, second_gain, second_gate, second_up, second_down
    )
    width = residual.shape[1] // lax.axis_size("tp")
    return lax.dynamic_slice_in_dim(residual, lax.axis_index("tp") * width, width, 1).astype(
        jnp.bfloat16
    )


def solution(mesh):
    placed = (
        P(None, ("kv", "tp")),
        P("kv"),
        P("kv", "tp"),
        P("kv", "tp"),
        P("tp", "kv"),
        P("kv"),
        P("kv", "tp"),
        P(None, "kv", "tp"),
        P(None, "kv", "tp"),
        P("tp"),
        P(),
        P("tp", "kv"),
        P("kv"),
        P("kv", "tp"),
        P("kv", "tp"),
        P("tp", "kv"),
    )
    return jax.shard_map(
        on_device, mesh=mesh, in_specs=placed, out_specs=P(None, ("kv", "tp")), check_vma=False
    )
```

profile of v0, /device:TPU:0, one launch (start us, length us, event | category | flops | bytes accessed | tf_op | source)
XLA Modules:
  0.0 626.8 jit_solution(4104942960489870407)
XLA Ops:
  6.5 6.5 %all_gather.39 = bf16[32,512]{1,0:T(8,128)(2,1)S(1)} all-gather(bf16[32,128]{1,0:T(8,128)(2,1)} %param.18), channel_id=1, replica_groups=mesh['kv'=8,'tp'=4] {'tp'}, dimensions={1}, use_global_device_ids=true | all-gather | bytes 40960 | tf_op jit(solution)/shard_map/all_gather | solution.py:124
  13.0 2.0 fusion.40
  15.0 1.4 fusion.42
  16.6 22.7 %psum.78 = f32[32,1]{0,1:T(1,128)S(1)} all-reduce(f32[32,1]{0,1:T(1,128)S(1)} %bitcast.79), channel_id=1, replica_groups=mesh['kv'=8,'tp'=4] {'kv'}, use_global_device_ids=true, to_apply=%region_2.0 | all-reduce | flops 32 | bytes 256 | tf_op jit(solution)/shard_map/psum | solution.py:22
  39.3 53.8 %all-reduce.19.cloned.1.call-done = (f32[32,2816]{1,0:T(8,128)}, f32[32,2816]{1,0:T(8,128)}) async-done(((f32[32,2816]{1,0:T(8,128)}, f32[32,2816]{1,0:T(8,128)}), (f32[32,2816]{1,0:T(8,128)}, f32[32,2816]{1,0:T(8,128)})) %all-reduce.19.cloned.1.call-update) | async-done | bytes 720912 | tf_op jit(solution)/shard_map/psum | solution.py:31
  93.1 2.4 fusion.28
  95.6 22.5 %copy.107 = bf16[32,1024,256]{1,2,0:T(8,128)(2,1)} copy(bf16[32,1024,256]{2,1,0:T(8,128)(2,1)} %param.25) | data formatting | bytes 33554432 | tf_op args[7]
  118.2 22.6 %copy.110 = bf16[32,1024,256]{1,2,0:T(8,128)(2,1)} copy(bf16[32,1024,256]{2,1,0:T(8,128)(2,1)} %param.26) | data formatting | bytes 33554432 | tf_op args[8]
  140.8 1.0 multiply_reduce_fusion.2
  141.7 19.6 %psum.82 = f32[32,1]{0,1:T(1,128)S(1)} all-reduce(f32[32,1]{0,1:T(1,128)S(1)} %bitcast.80), channel_id=1, replica_groups=mesh['kv'=8,'tp'=4] {'kv'}, use_global_device_ids=true, to_apply=%region_7.8 | all-reduce | flops 32 | bytes 256 | tf_op jit(solution)/shard_map/psum | solution.py:22
  161.3 1.7 fusion.38
  163.1 66.6 %all-reduce.11.cloned.1.call-done = f32[32,512]{1,0:T(8,128)} async-done(((f32[32,512]{1,0:T(8,128)}), f32[32,512]{1,0:T(8,128)}) %all-reduce.11.cloned.1.call-update) | async-done | bytes 65552 | tf_op jit(solution)/shard_map/psum | solution.py:60
  229.6 0.9 multiply_convert_fusion.6
  230.7 4.9 fusion.55
  235.6 4.9 fusion.54
  240.5 0.3 copy.108
  240.8 0.9 fusion.19
  241.7 0.3 copy.109
  242.0 30.9 %all-gather.1 = f32[256,4,2]{1,2,0:T(2,128)S(1)} all-gather(f32[32,4,2]{1,2,0:T(2,128)S(1)} %copy.109), channel_id=3, replica_groups=mesh['kv'=8,'tp'=4] {'kv'}, dimensions={0}, use_global_device_ids=true | all-gather | bytes 9216 | tf_op jit(solution)/shard_map/all_gather | solution.py:14
  272.9 0.3 copy.112
  273.2 1.0 fusion.21
  274.2 0.3 copy.113
  274.5 30.9 %all-gather.4 = f32[256,4,2]{1,2,0:T(2,128)S(1)} all-gather(f32[32,4,2]{1,2,0:T(2,128)S(1)} %copy.113), channel_id=6, replica_groups=mesh['kv'=8,'tp'=4] {'kv'}, dimensions={0}, use_global_device_ids=true | all-gather | bytes 9216 | tf_op jit(solution)/shard_map/all_gather | solution.py:14
  305.4 31.0 %all-gather = f32[256,4,2]{1,2,0:T(2,128)S(1)} all-gather(f32[32,4,2]{1,2,0:T(2,128)S(1)} %copy.108), channel_id=2, replica_groups=mesh['kv'=8,'tp'=4] {'kv'}, dimensions={0}, use_global_device_ids=true | all-gather | bytes 9216 | tf_op jit(solution)/shard_map/all_gather | solution.py:14
  336.4 0.8 slice.86
  337.1 31.1 %all-gather.3 = f32[256,4,2]{1,2,0:T(2,128)S(1)} all-gather(f32[32,4,2]{1,2,0:T(2,128)S(1)} %copy.112), channel_id=5, replica_groups=mesh['kv'=8,'tp'=4] {'kv'}, dimensions={0}, use_global_device_ids=true | all-gather | bytes 9216 | tf_op jit(solution)/shard_map/all_gather | solution.py:14
  368.2 0.8 slice.89
  369.0 8.8 %fusion.22 = f32[32,4,2,64]{3,2,1,0:T(2,128)} fusion(bf16[32,1024,4,64]{1,3,2,0:T(8,128)(2,1)} %bitcast.68, f32[32,4,2,1024]{3,2,1,0:T(2,128)S(1)} %get-tuple-element.178, f32[32,4,2]{2,1,0:T(4,128)S(1)} %get-tuple-element.177), kind=kOutput, calls=%fused_computation.32 | convolution fusion | flops 34078720 | bytes 17892352 | tf_op jit(solution)/shard_map/bkgp,bpkd->bkgd/dot_general | solution.py:79
  377.8 8.2 %fusion.24 = f32[32,4,2,64]{3,2,1,0:T(2,128)S(1)} fusion(bf16[32,1024,4,64]{1,3,2,0:T(8,128)(2,1)} %bitcast.69, f32[32,4,2,1024]{3,2,1,0:T(2,128)S(1)} %get-tuple-element.176, f32[32,4,2]{2,1,0:T(4,128)S(1)} %get-tuple-element.175), kind=kOutput, calls=%fused_computation.33 | convolution fusion | flops 34078720 | bytes 17892352 | tf_op jit(solution)/shard_map/bkgp,bpkd->bkgd/dot_general | solution.py:79
  386.0 32.9 %all-gather.5 = f32[256,4,2,64]{3,1,2,0:T(4,128)S(1)} all-gather(f32[32,4,2,64]{3,1,2,0:T(4,128)S(1)} %copy.114), channel_id=7, replica_groups=mesh['kv'=8,'tp'=4] {'kv'}, dimensions={0}, use_global_device_ids=true | all-gather | bytes 589824 | tf_op jit(solution)/shard_map/all_gather | solution.py:14
  418.9 0.7 slice.85
  419.6 0.2 slice.91
  419.8 32.1 %all-gather.2 = f32[256,4,2,64]{3,1,2,0:T(4,128)S(1)} all-gather(f32[32,4,2,64]{3,1,2,0:T(4,128)S(1)} %copy.111), channel_id=4, replica_groups=mesh['kv'=8,'tp'=4] {'kv'}, dimensions={0}, use_global_device_ids=true | all-gather | bytes 589824 | tf_op jit(solution)/shard_map/all_gather | solution.py:14
  451.8 0.7 slice.80
  452.5 0.2 slice.88
  452.8 0.1 copy.126
  453.0 0.1 copy.129
  453.3 1.1 copy.125
  454.5 1.1 copy.128
  455.5 1.0 copy.124
  456.5 1.0 copy.121
  457.6 11.1 %while.20 = (s32[]{:T(128)}, f32[32,4,2]{0,2,1:T(2,128)S(1)}, f32[32,4,2]{0,2,1:T(2,128)S(1)}, f32[32,4,2,64]{3,2,1,0:T(2,128)S(1)}, f32[32,4,2]{0,2,1:T(2,128)S...) while((s32[]{:T(128)}, f32[32,4,2]{0,2,1:T(2,128)S(1)}, ...), condition=%wide.region_13.14_spmd, body=%wide.region_12.13_spmd.sunk | while | flops 101378 | bytes 684189 | solution.py:17
  458.2 1.0 fusion.73
  459.7 1.0 fusion.73
  461.3 1.0 fusion.73
  462.9 1.0 fusion.73
  464.5 1.0 fusion.73
  466.1 1.0 fusion.73
  467.6 1.0 fusion.73
  468.7 0.1 copy.131
  468.9 0.6 multiply_reduce_fusion
  469.5 0.1 copy.134
  469.7 0.2 multiply_convert_fusion.4
  469.9 0.1 reshape.36
  470.0 0.8 fusion.56
  470.9 31.2 %all-reduce.13.cloned.1.call-done = f32[32,512]{1,0:T(8,128)} async-done(((f32[32,512]{1,0:T(8,128)}), f32[32,512]{1,0:T(8,128)}) %all-reduce.13.cloned.1.call-update) | async-done | bytes 65552 | tf_op jit(solution)/shard_map/psum | solution.py:103
  502.1 1.0 multiply_reduce_fusion.1
  503.1 3.1 fusion.46
  506.2 3.3 fusion.47
  509.6 21.5 %psum.85 = f32[32,1]{0,1:T(1,128)S(1)} all-reduce(f32[32,1]{0,1:T(1,128)S(1)} %bitcast.78), channel_id=1, replica_groups=mesh['kv'=8,'tp'=4] {'kv'}, use_global_device_ids=true, to_apply=%region_18.19 | all-reduce | flops 32 | bytes 256 | tf_op jit(solution)/shard_map/psum | solution.py:22
  531.1 53.4 %all-reduce.17.cloned.1.call-done = (f32[32,2816]{1,0:T(8,128)}, f32[32,2816]{1,0:T(8,128)}) async-done(((f32[32,2816]{1,0:T(8,128)}, f32[32,2816]{1,0:T(8,128)}), (f32[32,2816]{1,0:T(8,128)}, f32[32,2816]{1,0:T(8,128)})) %all-reduce.17.cloned.1.call-update) | async-done | bytes 720912 | tf_op jit(solution)/shard_map/psum | solution.py:31
  584.5 3.3 fusion.29
  587.8 30.8 %all-reduce.15.cloned.1.call-done = f32[32,512]{1,0:T(8,128)} async-done(((f32[32,512]{1,0:T(8,128)}), f32[32,512]{1,0:T(8,128)}) %all-reduce.15.cloned.1.call-update) | async-done | bytes 65552 | tf_op jit(solution)/shard_map/psum | solution.py:35
  618.7 1.3 fusion.45
  (130 shorter events, 5.3 us)
Async XLA Ops:
  6.5 6.5 %copy-start = (bf16[512,2816]{1,0:T(8,128)(2,1)S(1)}, bf16[512,2816]{1,0:T(8,128)(2,1)}, u32[]{:S(2)}) copy-start(bf16[512,2816]{1,0:T(8,128)(2,1)} %param.21) | copy-start | bytes 8650756
  6.5 8.5 %copy-start.12 = (f32[512]{0:T(512)S(1)}, f32[512]{0:T(512)}, u32[]{:S(2)}) copy-start(f32[512]{0:T(512)} %param.19) | copy-start | bytes 6148
  6.5 86.6 %all-reduce.19.cloned.1.call-start = ((), (), s32[]{:S(2)}) async-start(), calls=%async_computation.5 | async-start | bytes 1441792 | tf_op jit(solution)/shard_map/psum | solution.py:31
  6.5 8.5 %copy-start.2 = (bf16[512,2816]{1,0:T(8,128)(2,1)S(1)}, bf16[512,2816]{1,0:T(8,128)(2,1)}, u32[]{:S(2)}) copy-start(bf16[512,2816]{1,0:T(8,128)(2,1)} %param.20) | copy-start | bytes 8650756
  15.0 78.1 %copy-start.3 = (bf16[2816,512]{1,0:T(8,128)(2,1)S(1)}, bf16[2816,512]{1,0:T(8,128)(2,1)}, u32[]{:S(2)}) copy-start(bf16[2816,512]{1,0:T(8,128)(2,1)} %param.22) | copy-start | bytes 8650756
  16.4 79.2 %copy-start.16 = (f32[8]{0:T(128)S(1)}, f32[8]{0:T(128)}, u32[]{:S(2)}) copy-start(f32[8]{0:T(128)} %param.27) | copy-start | bytes 100
  16.4 124.3 %all-reduce.9.cloned.1.call-start = ((), (), s32[]{:S(2)}) async-start(), calls=%async_computation | async-start | bytes 131072 | tf_op jit(solution)/shard_map/psum | solution.py:35
  95.5 134.1 %all-reduce.11.cloned.1.call-start = ((), (), s32[]{:S(2)}) async-start(), calls=%async_computation.1 | async-start | bytes 131072 | tf_op jit(solution)/shard_map/psum | solution.py:60
  118.2 43.1 %copy-start.10 = (bf16[512,512]{1,0:T(8,128)(2,1)S(1)}, bf16[512,512]{1,0:T(8,128)(2,1)}, u32[]{:S(2)}) copy-start(bf16[512,512]{1,0:T(8,128)(2,1)} %param.24) | copy-start | bytes 1572868
  118.2 43.1 %copy-start.14 = (f32[512]{0:T(512)S(1)}, f32[512]{0:T(512)}, u32[]{:S(2)}) copy-start(f32[512]{0:T(512)} %param.23) | copy-start | bytes 6148
  163.0 339.1 %all-reduce.13.cloned.1.call-start = ((), (), s32[]{:S(2)}) async-start(), calls=%async_computation.2 | async-start | bytes 131072 | tf_op jit(solution)/shard_map/psum | solution.py:103
  272.9 104.9 %copy-start.4 = (f32[256,4,2]{1,2,0:T(2,128)}, f32[256,4,2]{1,2,0:T(2,128)S(1)}, u32[]{:S(2)}) copy-start(f32[256,4,2]{1,2,0:T(2,128)S(1)} %all-gather.1) | copy-start | bytes 24580
  305.4 72.4 %copy-start.5 = (f32[256,4,2]{1,2,0:T(2,128)}, f32[256,4,2]{1,2,0:T(2,128)S(1)}, u32[]{:S(2)}) copy-start(f32[256,4,2]{1,2,0:T(2,128)S(1)} %all-gather.4) | copy-start | bytes 24580
  336.4 41.4 %copy-start.6 = (f32[256,4,2]{1,2,0:T(2,128)}, f32[256,4,2]{1,2,0:T(2,128)S(1)}, u32[]{:S(2)}) copy-start(f32[256,4,2]{1,2,0:T(2,128)S(1)} %all-gather) | copy-start | bytes 24580
  368.2 9.6 %copy-start.7 = (f32[256,4,2]{1,2,0:T(2,128)}, f32[256,4,2]{1,2,0:T(2,128)S(1)}, u32[]{:S(2)}) copy-start(f32[256,4,2]{1,2,0:T(2,128)S(1)} %all-gather.3) | copy-start | bytes 24580
  377.8 8.2 %copy-start.11 = (f32[32,4,2,64]{3,2,1,0:T(2,128)S(1)}, f32[32,4,2,64]{3,2,1,0:T(2,128)}, u32[]{:S(2)}) copy-start(f32[32,4,2,64]{3,2,1,0:T(2,128)} %fusion.22) | copy-start | bytes 196612
  418.9 33.8 %slice-start = ((f32[256,4,2]{1,2,0:T(2,128)}), f32[32,4,2]{1,2,0:T(2,128)S(1)}, s32[]{:S(2)}) async-start(f32[256,4,2]{1,2,0:T(2,128)} %copy-done.4), calls=%async_computation.6 | async-start | bytes 65536 | tf_op jit(solution)/shard_map/slice | solution.py:15
  418.9 33.9 %slice-start.1 = ((f32[256,4,2]{1,2,0:T(2,128)}), f32[224,4,2]{1,2,0:T(2,128)S(1)}, s32[]{:S(2)}) async-start(f32[256,4,2]{1,2,0:T(2,128)} %copy-done.4), calls=%async_computation.7 | async-start | bytes 458752 | tf_op jit(solution)/shard_map/slice | solution.py:16
  419.5 33.4 %slice-start.2 = ((f32[256,4,2]{1,2,0:T(2,128)}), f32[32,4,2]{1,2,0:T(2,128)S(1)}, s32[]{:S(2)}) async-start(f32[256,4,2]{1,2,0:T(2,128)} %copy-done.5), calls=%async_computation.8 | async-start | bytes 65536 | tf_op jit(solution)/shard_map/slice | solution.py:15
  419.6 33.5 %slice-start.3 = ((f32[256,4,2]{1,2,0:T(2,128)}), f32[224,4,2]{1,2,0:T(2,128)S(1)}, s32[]{:S(2)}) async-start(f32[256,4,2]{1,2,0:T(2,128)} %copy-done.5), calls=%async_computation.9 | async-start | bytes 458752 | tf_op jit(solution)/shard_map/slice | solution.py:16
  419.6 33.6 %slice-start.4 = ((f32[256,4,2]{1,2,0:T(2,128)}), f32[32,4,2]{1,2,0:T(2,128)S(1)}, s32[]{:S(2)}) async-start(f32[256,4,2]{1,2,0:T(2,128)} %copy-done.6), calls=%async_computation.10 | async-start | bytes 65536 | tf_op jit(solution)/shard_map/slice | solution.py:15
  419.6 34.8 %slice-start.5 = ((f32[256,4,2]{1,2,0:T(2,128)}), f32[32,4,2]{1,2,0:T(2,128)S(1)}, s32[]{:S(2)}) async-start(f32[256,4,2]{1,2,0:T(2,128)} %copy-done.7), calls=%async_computation.11 | async-start | bytes 65536 | tf_op jit(solution)/shard_map/slice | solution.py:15
  457.5 12.1 %copy-start.15 = (f32[64]{0:T(128)S(1)}, f32[64]{0:T(128)}, u32[]{:S(2)}) copy-start(f32[64]{0:T(128)} %param.28) | copy-start | bytes 772
  457.5 12.5 %copy-start.9 = (bf16[512,512]{1,0:T(8,128)(2,1)S(1)}, bf16[512,512]{1,0:T(8,128)(2,1)}, u32[]{:S(2)}) copy-start(bf16[512,512]{1,0:T(8,128)(2,1)} %param.29) | copy-start | bytes 1572868
  457.5 44.6 %copy-start.8 = (f32[32,512]{1,0:T(8,128)S(1)}, f32[32,512]{1,0:T(8,128)}, u32[]{:S(2)}) copy-start(f32[32,512]{1,0:T(8,128)} %all-reduce.9.cloned.1.call-done) | copy-start | bytes 196612
  457.6 45.5 %copy-start.13 = (f32[512]{0:T(512)S(1)}, f32[512]{0:T(512)}, u32[]{:S(2)}) copy-start(f32[512]{0:T(512)} %param.30) | copy-start | bytes 6148
  470.9 113.6 %all-reduce.17.cloned.1.call-start = ((), (), s32[]{:S(2)}) async-start(), calls=%async_computation.4 | async-start | bytes 1441792 | tf_op jit(solution)/shard_map/psum | solution.py:31
  506.2 113.8 %copy-start.1 = (bf16[512,2816]{1,0:T(8,128)(2,1)S(1)}, bf16[512,2816]{1,0:T(8,128)(2,1)}, u32[]{:S(2)}) copy-start(bf16[512,2816]{1,0:T(8,128)(2,1)} %param.21) | copy-start | bytes 8650756
  509.6 109.1 %all-reduce.15.cloned.1.call-start = ((), (), s32[]{:S(2)}) async-start(), calls=%async_computation.3 | async-start | bytes 131072 | tf_op jit(solution)/shard_map/psum | solution.py:35
Sparse Core Ops, SparseCore 0:
  16.5 76.5 all-reduce.18
  95.6 30.6 all-reduce.8
  163.1 66.4 all-reduce.10
  471.0 31.0 all-reduce.12
  509.7 74.7 all-reduce.16
  588.0 30.6 all-reduce.14
where the time goes:
time: 629 us; the launch traced here: 627 us
  blocking collectives  259 us (41%)
  waiting for transfers between devices  236 us (38%)
  local copies, waits for them, and re-layouts  58.6 us (9%)
  matrix products  44.7 us (7%)
  other arithmetic  14.3 us (2%)
  between operations  13.7 us (2%)
    all_gather x6, blocking collectives, merged(): pieces = jax.tree.map(lambda part: lax.all_gather(part, axis), value)  189 us
    psum x2, waiting for transfers between devices, channel_mixer(): gate_sum, up_sum = lax.psum((part_gate, part_up), 'kv')  107 us
    psum x1, waiting for transfers between devices, attention_mix(): queries = lax.psum(part_query, 'kv')  66.6 us
    psum x3, blocking collectives, norm_total(): return lax.psum(squares, 'kv')  63.8 us
    unnamed x36, local copies, waits for them, and re-layouts  45.2 us
    psum x1, waiting for transfers between devices, attention_mix(): return lax.psum(partial_value, 'tp')  31.2 us
    psum x2, waiting for transfers between devices, channel_mixer(): return lax.psum(partial_value, 'tp')  30.8 us
    dot_general x2, matrix products, partial_map(): jnp.einsum('bkgp,bpkd->bkgd', exp_terms.astype(jnp.bfloat16), stored, pre...  16.9 us
  transfers between devices with their start and end apart: 6, of which 5 were waited for; matrix products, arithmetic and copies ran while one was open for 7% of the time, Pallas kernels for 0%

commit v1 on v0

--- a/solution.py
+++ b/solution.py
@@ -57,7 +57,7 @@
     scaled = (residual * mix_gain).astype(jnp.bfloat16)
     part_query = jnp.dot(scaled, w_query, preferred_element_type=jnp.float32)
     row_total = norm_total(squares)
-    queries = lax.psum(part_query, "kv")
+    queries = jnp.sum(lax.all_gather(part_query, "kv"), axis=0)
     queries = (queries * lax.rsqrt(row_total / D + EPS)).astype(jnp.bfloat16)
     batch_rows = queries.shape[0]
     kv_local = key_cache.shape[2] // HEAD

time: 629 us -> 589 us (0.936)
  waiting for transfers between devices: 236 us -> 167 us
  blocking collectives: 259 us -> 290 us
    psum x1 -> x0, waiting for transfers between devices: 66.6 us -> none  [attention_mix(): queries = lax.psum(part_query, 'kv')]
    all_gather x0 -> x1, blocking collectives: none -> 31.5 us  [attention_mix(): queries = jnp.sum(lax.all_gather(part_query, 'kv'), axis=0)]
  transfers between devices with their start and end apart: 6 -> 5, of which waited for: 5 -> 4; matrix products, arithmetic and copies ran while one was open for 7% -> 8% of each run, Pallas kernels for 0% -> 0%
where the time goes in v1:
time: 589 us; the launch traced here: 587 us
  blocking collectives  290 us (49%)
  waiting for transfers between devices  167 us (28%)
  local copies, waits for them, and re-layouts  58.7 us (10%)
  matrix products  44.1 us (7%)
  other arithmetic  13.5 us (2%)
  between operations  13.4 us (2%)
    all_gather x6, blocking collectives, merged(): pieces = jax.tree.map(lambda part: lax.all_gather(part, axis), value)  188 us
    psum x2, waiting for transfers between devices, channel_mixer(): gate_sum, up_sum = lax.psum((part_gate, part_up), 'kv')  107 us
    psum x3, blocking collectives, norm_total(): return lax.psum(squares, 'kv')  63.9 us
    unnamed x36, local copies, waits for them, and re-layouts  45.2 us
    all_gather x1, blocking collectives, attention_mix(): queries = jnp.sum(lax.all_gather(part_query, 'kv'), axis=0)  31.5 us
    psum x2, waiting for transfers between devices, channel_mixer(): return lax.psum(partial_value, 'tp')  30.8 us
    psum x1, waiting for transfers between devices, attention_mix(): return lax.psum(partial_value, 'tp')  28.9 us
    dot_general x2, matrix products, partial_map(): jnp.einsum('bkgp,bpkd->bkgd', exp_terms.astype(jnp.bfloat16), stored, pre...  16.9 us
  transfers between devices with their start and end apart: 5, of which 4 were waited for; matrix products, arithmetic and copies ran while one was open for 8% of the time, Pallas kernels for 0%

profile of v1, /device:TPU:0, one launch (start us, length us, event | category | flops | bytes accessed | tf_op | source)
XLA Modules:
  0.0 587.1 jit_solution(9557516011567195346)
XLA Ops:
  6.5 6.5 %all_gather.45 = bf16[32,512]{1,0:T(8,128)(2,1)S(1)} all-gather(bf16[32,128]{1,0:T(8,128)(2,1)} %param.18), channel_id=1, replica_groups=mesh['kv'=8,'tp'=4] {'tp'}, dimensions={1}, use_global_device_ids=true | all-gather | bytes 40960 | tf_op jit(solution)/shard_map/all_gather | solution.py:124
  13.0 2.0 fusion.40
  15.1 1.3 fusion.42
  16.6 22.7 %psum.71 = f32[32,1]{0,1:T(1,128)S(1)} all-reduce(f32[32,1]{0,1:T(1,128)S(1)} %bitcast.81), channel_id=1, replica_groups=mesh['kv'=8,'tp'=4] {'kv'}, use_global_device_ids=true, to_apply=%region_2.0 | all-reduce | flops 32 | bytes 256 | tf_op jit(solution)/shard_map/psum | solution.py:22
  39.3 53.8 %all-reduce.16.cloned.1.call-done = (f32[32,2816]{1,0:T(8,128)}, f32[32,2816]{1,0:T(8,128)}) async-done(((f32[32,2816]{1,0:T(8,128)}, f32[32,2816]{1,0:T(8,128)}), (f32[32,2816]{1,0:T(8,128)}, f32[32,2816]{1,0:T(8,128)})) %all-reduce.16.cloned.1.call-update) | async-done | bytes 720912 | tf_op jit(solution)/shard_map/psum | solution.py:31
  93.1 2.4 fusion.28
  95.6 22.6 %copy.107 = bf16[32,1024,256]{1,2,0:T(8,128)(2,1)} copy(bf16[32,1024,256]{2,1,0:T(8,128)(2,1)} %param.25) | data formatting | bytes 33554432 | tf_op args[7]
  118.2 22.6 %copy.110 = bf16[32,1024,256]{1,2,0:T(8,128)(2,1)} copy(bf16[32,1024,256]{2,1,0:T(8,128)(2,1)} %param.26) | data formatting | bytes 33554432 | tf_op args[8]
  140.8 1.0 multiply_reduce_fusion.2
  141.7 19.6 %psum.74 = f32[32,1]{0,1:T(1,128)S(1)} all-reduce(f32[32,1]{0,1:T(1,128)S(1)} %bitcast.82), channel_id=1, replica_groups=mesh['kv'=8,'tp'=4] {'kv'}, use_global_device_ids=true, to_apply=%region_7.8 | all-reduce | flops 32 | bytes 256 | tf_op jit(solution)/shard_map/psum | solution.py:22
  161.3 1.0 fusion.38
  162.4 31.5 %all-gather = f32[256,512]{1,0:T(8,128)S(1)} all-gather(f32[32,512]{1,0:T(8,128)S(1)} %fusion.38), channel_id=2, replica_groups=mesh['kv'=8,'tp'=4] {'kv'}, dimensions={0}, use_global_device_ids=true | all-gather | bytes 589824 | tf_op jit(solution)/shard_map/all_gather | solution.py:60
  193.9 0.1 reduce_sum.67
  194.2 4.9 fusion.55
  199.1 4.9 fusion.54
  204.0 0.3 copy.108
  204.3 0.9 fusion.19
  205.3 0.3 copy.109
  205.6 30.9 %all-gather.2 = f32[256,4,2]{1,2,0:T(2,128)S(1)} all-gather(f32[32,4,2]{1,2,0:T(2,128)S(1)} %copy.109), channel_id=4, replica_groups=mesh['kv'=8,'tp'=4] {'kv'}, dimensions={0}, use_global_device_ids=true | all-gather | bytes 9216 | tf_op jit(solution)/shard_map/all_gather | solution.py:14
  236.4 0.3 copy.112
  236.8 1.0 fusion.21
  237.7 0.3 copy.113
  238.0 30.7 %all-gather.5 = f32[256,4,2]{1,2,0:T(2,128)S(1)} all-gather(f32[32,4,2]{1,2,0:T(2,128)S(1)} %copy.113), channel_id=7, replica_groups=mesh['kv'=8,'tp'=4] {'kv'}, dimensions={0}, use_global_device_ids=true | all-gather | bytes 9216 | tf_op jit(solution)/shard_map/all_gather | solution.py:14
  268.7 30.8 %all-gather.1 = f32[256,4,2]{1,2,0:T(2,128)S(1)} all-gather(f32[32,4,2]{1,2,0:T(2,128)S(1)} %copy.108), channel_id=3, replica_groups=mesh['kv'=8,'tp'=4] {'kv'}, dimensions={0}, use_global_device_ids=true | all-gather | bytes 9216 | tf_op jit(solution)/shard_map/all_gather | solution.py:14
  299.5 0.8 slice.86
  300.3 31.0 %all-gather.4 = f32[256,4,2]{1,2,0:T(2,128)S(1)} all-gather(f32[32,4,2]{1,2,0:T(2,128)S(1)} %copy.112), channel_id=6, replica_groups=mesh['kv'=8,'tp'=4] {'kv'}, dimensions={0}, use_global_device_ids=true | all-gather | bytes 9216 | tf_op jit(solution)/shard_map/all_gather | solution.py:14
  331.3 0.8 slice.89
  332.0 8.8 %fusion.22 = f32[32,4,2,64]{3,2,1,0:T(2,128)} fusion(bf16[32,1024,4,64]{1,3,2,0:T(8,128)(2,1)} %bitcast.69, f32[32,4,2,1024]{3,2,1,0:T(2,128)S(1)} %get-tuple-element.178, f32[32,4,2]{2,1,0:T(4,128)S(1)} %get-tuple-element.177), kind=kOutput, calls=%fused_computation.32 | convolution fusion | flops 34078720 | bytes 17892352 | tf_op jit(solution)/shard_map/bkgp,bpkd->bkgd/dot_general | solution.py:79
  340.8 8.2 %fusion.24 = f32[32,4,2,64]{3,2,1,0:T(2,128)S(1)} fusion(bf16[32,1024,4,64]{1,3,2,0:T(8,128)(2,1)} %bitcast.70, f32[32,4,2,1024]{3,2,1,0:T(2,128)S(1)} %get-tuple-element.176, f32[32,4,2]{2,1,0:T(4,128)S(1)} %get-tuple-element.175), kind=kOutput, calls=%fused_computation.33 | convolution fusion | flops 34078720 | bytes 17892352 | tf_op jit(solution)/shard_map/bkgp,bpkd->bkgd/dot_general | solution.py:79
  349.0 32.5 %all-gather.6 = f32[256,4,2,64]{3,1,2,0:T(4,128)S(1)} all-gather(f32[32,4,2,64]{3,1,2,0:T(4,128)S(1)} %copy.114), channel_id=8, replica_groups=mesh['kv'=8,'tp'=4] {'kv'}, dimensions={0}, use_global_device_ids=true | all-gather | bytes 589824 | tf_op jit(solution)/shard_map/all_gather | solution.py:14
  381.5 0.7 slice.85
  382.2 0.2 slice.91
  382.4 32.6 %all-gather.3 = f32[256,4,2,64]{3,1,2,0:T(4,128)S(1)} all-gather(f32[32,4,2,64]{3,1,2,0:T(4,128)S(1)} %copy.111), channel_id=5, replica_groups=mesh['kv'=8,'tp'=4] {'kv'}, dimensions={0}, use_global_device_ids=true | all-gather | bytes 589824 | tf_op jit(solution)/shard_map/all_gather | solution.py:14
  415.0 0.7 slice.80
  415.6 0.2 slice.88
  415.9 0.1 copy.126
  416.2 0.1 copy.129
  416.4 1.1 copy.125
  417.6 1.1 copy.128
  418.7 1.0 copy.124
  419.7 1.0 copy.121
  420.7 11.1 %while.20 = (s32[]{:T(128)}, f32[32,4,2]{0,2,1:T(2,128)S(1)}, f32[32,4,2]{0,2,1:T(2,128)S(1)}, f32[32,4,2,64]{3,2,1,0:T(2,128)S(1)}, f32[32,4,2]{0,2,1:T(2,128)S...) while((s32[]{:T(128)}, f32[32,4,2]{0,2,1:T(2,128)S(1)}, ...), condition=%wide.region_13.14_spmd, body=%wide.region_12.13_spmd.sunk | while | flops 101378 | bytes 684189 | solution.py:17
  421.3 1.0 fusion.73
  422.9 1.0 fusion.73
  424.5 1.0 fusion.73
  426.0 1.0 fusion.73
  427.6 1.0 fusion.73
  429.2 1.0 fusion.73
  430.4 0.1 copy.163
  430.8 1.0 fusion.73
  432.0 0.6 multiply_reduce_fusion
  432.7 0.1 copy.134
  432.8 0.2 multiply_convert_fusion.4
  433.0 0.1 reshape.39
  433.2 0.8 fusion.56
  434.0 28.9 %all-reduce.10.cloned.1.call-done = f32[32,512]{1,0:T(8,128)} async-done(((f32[32,512]{1,0:T(8,128)}), f32[32,512]{1,0:T(8,128)}) %all-reduce.10.cloned.1.call-update) | async-done | bytes 65552 | tf_op jit(solution)/shard_map/psum | solution.py:103
  462.9 1.0 multiply_reduce_fusion.1
  463.9 3.1 fusion.46
  467.0 3.3 fusion.47
  470.4 21.6 %psum.77 = f32[32,1]{0,1:T(1,128)S(1)} all-reduce(f32[32,1]{0,1:T(1,128)S(1)} %bitcast.80), channel_id=1, replica_groups=mesh['kv'=8,'tp'=4] {'kv'}, use_global_device_ids=true, to_apply=%region_18.19 | all-reduce | flops 32 | bytes 256 | tf_op jit(solution)/shard_map/psum | solution.py:22
  492.0 53.1 %all-reduce.14.cloned.1.call-done = (f32[32,2816]{1,0:T(8,128)}, f32[32,2816]{1,0:T(8,128)}) async-done(((f32[32,2816]{1,0:T(8,128)}, f32[32,2816]{1,0:T(8,128)}), (f32[32,2816]{1,0:T(8,128)}, f32[32,2816]{1,0:T(8,128)})) %all-reduce.14.cloned.1.call-update) | async-done | bytes 720912 | tf_op jit(solution)/shard_map/psum | solution.py:31
  545.1 3.3 fusion.29
  548.5 30.8 %all-reduce.12.cloned.1.call-done = f32[32,512]{1,0:T(8,128)} async-done(((f32[32,512]{1,0:T(8,128)}), f32[32,512]{1,0:T(8,128)}) %all-reduce.12.cloned.1.call-update) | async-done | bytes 65552 | tf_op jit(solution)/shard_map/psum | solution.py:35
  579.3 1.3 fusion.45
  (129 shorter events, 5.3 us)
Async XLA Ops:
  6.5 6.5 %copy-start = (bf16[512,2816]{1,0:T(8,128)(2,1)S(1)}, bf16[512,2816]{1,0:T(8,128)(2,1)}, u32[]{:S(2)}) copy-start(bf16[512,2816]{1,0:T(8,128)(2,1)} %param.21) | copy-start | bytes 8650756
  6.5 8.5 %copy-start.12 = (f32[512]{0:T(512)S(1)}, f32[512]{0:T(512)}, u32[]{:S(2)}) copy-start(f32[512]{0:T(512)} %param.19) | copy-start | bytes 6148
  6.5 86.5 %all-reduce.16.cloned.1.call-start = ((), (), s32[]{:S(2)}) async-start(), calls=%async_computation.4 | async-start | bytes 1441792 | tf_op jit(solution)/shard_map/psum | solution.py:31
  6.5 8.5 %copy-start.2 = (bf16[512,2816]{1,0:T(8,128)(2,1)S(1)}, bf16[512,2816]{1,0:T(8,128)(2,1)}, u32[]{:S(2)}) copy-start(bf16[512,2816]{1,0:T(8,128)(2,1)} %param.20) | copy-start | bytes 8650756
  15.1 78.0 %copy-start.3 = (bf16[2816,512]{1,0:T(8,128)(2,1)S(1)}, bf16[2816,512]{1,0:T(8,128)(2,1)}, u32[]{:S(2)}) copy-start(bf16[2816,512]{1,0:T(8,128)(2,1)} %param.22) | copy-start | bytes 8650756
  16.4 79.1 %copy-start.16 = (f32[8]{0:T(128)S(1)}, f32[8]{0:T(128)}, u32[]{:S(2)}) copy-start(f32[8]{0:T(128)} %param.27) | copy-start | bytes 100
  16.4 124.3 %all-reduce.8.cloned.1.call-start = ((), (), s32[]{:S(2)}) async-start(), calls=%async_computation | async-start | bytes 131072 | tf_op jit(solution)/shard_map/psum | solution.py:35
  95.5 367.4 %all-reduce.10.cloned.1.call-start = ((), (), s32[]{:S(2)}) async-start(), calls=%async_computation.1 | async-start | bytes 131072 | tf_op jit(solution)/shard_map/psum | solution.py:103
  118.2 43.2 %copy-start.10 = (bf16[512,512]{1,0:T(8,128)(2,1)S(1)}, bf16[512,512]{1,0:T(8,128)(2,1)}, u32[]{:S(2)}) copy-start(bf16[512,512]{1,0:T(8,128)(2,1)} %param.24) | copy-start | bytes 1572868
  118.2 43.2 %copy-start.14 = (f32[512]{0:T(512)S(1)}, f32[512]{0:T(512)}, u32[]{:S(2)}) copy-start(f32[512]{0:T(512)} %param.23) | copy-start | bytes 6148
  236.4 104.4 %copy-start.4 = (f32[256,4,2]{1,2,0:T(2,128)}, f32[256,4,2]{1,2,0:T(2,128)S(1)}, u32[]{:S(2)}) copy-start(f32[256,4,2]{1,2,0:T(2,128)S(1)} %all-gather.2) | copy-start | bytes 24580
  268.7 72.1 %copy-start.5 = (f32[256,4,2]{1,2,0:T(2,128)}, f32[256,4,2]{1,2,0:T(2,128)S(1)}, u32[]{:S(2)}) copy-start(f32[256,4,2]{1,2,0:T(2,128)S(1)} %all-gather.5) | copy-start | bytes 24580
  299.5 41.3 %copy-start.6 = (f32[256,4,2]{1,2,0:T(2,128)}, f32[256,4,2]{1,2,0:T(2,128)S(1)}, u32[]{:S(2)}) copy-start(f32[256,4,2]{1,2,0:T(2,128)S(1)} %all-gather.1) | copy-start | bytes 24580
  331.3 9.5 %copy-start.7 = (f32[256,4,2]{1,2,0:T(2,128)}, f32[256,4,2]{1,2,0:T(2,128)S(1)}, u32[]{:S(2)}) copy-start(f32[256,4,2]{1,2,0:T(2,128)S(1)} %all-gather.4) | copy-start | bytes 24580
  340.8 8.2 %copy-start.11 = (f32[32,4,2,64]{3,2,1,0:T(2,128)S(1)}, f32[32,4,2,64]{3,2,1,0:T(2,128)}, u32[]{:S(2)}) copy-start(f32[32,4,2,64]{3,2,1,0:T(2,128)} %fusion.22) | copy-start | bytes 196612
  381.5 34.3 %slice-start = ((f32[256,4,2]{1,2,0:T(2,128)}), f32[32,4,2]{1,2,0:T(2,128)S(1)}, s32[]{:S(2)}) async-start(f32[256,4,2]{1,2,0:T(2,128)} %copy-done.4), calls=%async_computation.5 | async-start | bytes 65536 | tf_op jit(solution)/shard_map/slice | solution.py:15
  381.5 34.4 %slice-start.1 = ((f32[256,4,2]{1,2,0:T(2,128)}), f32[224,4,2]{1,2,0:T(2,128)S(1)}, s32[]{:S(2)}) async-start(f32[256,4,2]{1,2,0:T(2,128)} %copy-done.4), calls=%async_computation.6 | async-start | bytes 458752 | tf_op jit(solution)/shard_map/slice | solution.py:16
  382.2 33.8 %slice-start.2 = ((f32[256,4,2]{1,2,0:T(2,128)}), f32[32,4,2]{1,2,0:T(2,128)S(1)}, s32[]{:S(2)}) async-start(f32[256,4,2]{1,2,0:T(2,128)} %copy-done.5), calls=%async_computation.7 | async-start | bytes 65536 | tf_op jit(solution)/shard_map/slice | solution.py:15
  382.2 33.9 %slice-start.3 = ((f32[256,4,2]{1,2,0:T(2,128)}), f32[224,4,2]{1,2,0:T(2,128)S(1)}, s32[]{:S(2)}) async-start(f32[256,4,2]{1,2,0:T(2,128)} %copy-done.5), calls=%async_computation.8 | async-start | bytes 458752 | tf_op jit(solution)/shard_map/slice | solution.py:16
  382.2 34.1 %slice-start.4 = ((f32[256,4,2]{1,2,0:T(2,128)}), f32[32,4,2]{1,2,0:T(2,128)S(1)}, s32[]{:S(2)}) async-start(f32[256,4,2]{1,2,0:T(2,128)} %copy-done.6), calls=%async_computation.9 | async-start | bytes 65536 | tf_op jit(solution)/shard_map/slice | solution.py:15
  382.2 35.3 %slice-start.5 = ((f32[256,4,2]{1,2,0:T(2,128)}), f32[32,4,2]{1,2,0:T(2,128)S(1)}, s32[]{:S(2)}) async-start(f32[256,4,2]{1,2,0:T(2,128)} %copy-done.7), calls=%async_computation.10 | async-start | bytes 65536 | tf_op jit(solution)/shard_map/slice | solution.py:15
  420.7 12.1 %copy-start.15 = (f32[64]{0:T(128)S(1)}, f32[64]{0:T(128)}, u32[]{:S(2)}) copy-start(f32[64]{0:T(128)} %param.28) | copy-start | bytes 772
  420.7 12.5 %copy-start.9 = (bf16[512,512]{1,0:T(8,128)(2,1)S(1)}, bf16[512,512]{1,0:T(8,128)(2,1)}, u32[]{:S(2)}) copy-start(bf16[512,512]{1,0:T(8,128)(2,1)} %param.29) | copy-start | bytes 1572868
  420.7 42.2 %copy-start.8 = (f32[32,512]{1,0:T(8,128)S(1)}, f32[32,512]{1,0:T(8,128)}, u32[]{:S(2)}) copy-start(f32[32,512]{1,0:T(8,128)} %all-reduce.8.cloned.1.call-done) | copy-start | bytes 196612
  420.7 43.2 %copy-start.13 = (f32[512]{0:T(512)S(1)}, f32[512]{0:T(512)}, u32[]{:S(2)}) copy-start(f32[512]{0:T(512)} %param.30) | copy-start | bytes 6148
  434.0 111.1 %all-reduce.14.cloned.1.call-start = ((), (), s32[]{:S(2)}) async-start(), calls=%async_computation.3 | async-start | bytes 1441792 | tf_op jit(solution)/shard_map/psum | solution.py:31
  467.0 113.6 %copy-start.1 = (bf16[512,2816]{1,0:T(8,128)(2,1)S(1)}, bf16[512,2816]{1,0:T(8,128)(2,1)}, u32[]{:S(2)}) copy-start(bf16[512,2816]{1,0:T(8,128)(2,1)} %param.21) | copy-start | bytes 8650756
  470.4 108.9 %all-reduce.12.cloned.1.call-start = ((), (), s32[]{:S(2)}) async-start(), calls=%async_computation.2 | async-start | bytes 131072 | tf_op jit(solution)/shard_map/psum | solution.py:35
Sparse Core Ops, SparseCore 0:
  16.5 76.4 all-reduce.15
  95.6 30.6 all-reduce.7
  434.1 28.7 all-reduce.9
  470.5 74.5 all-reduce.13
  548.6 30.6 all-reduce.11
